TPU v7x, 32 devices: a whole 2x2x4 slice. The times are simulated.
32 devices in a mesh: ep: 8 (over z, core), tp: 4 (over y, x).
Axes of the slice: x: 2, y: 2, z: 4, core: 2. Of those that a mesh axis runs over, the one named last changes fastest.
Arguments:
- tokens: bfloat16 [512, 2048], P('ep', 'tp'), may hold values from -20 to 20
- state: float32 [512, 16, 64, 64], P('ep', 'tp'), may hold values from -1.5 to 1.5
- attn_gain: float32 [2048], replicated, may hold values from 0.1 to 1.9
- ffn_gain: float32 [2048], replicated, may hold values from 0.1 to 1.9
- w_query: bfloat16 [2048, 1024], P(None, 'tp'), may hold values from -0.125 to 0.125
- w_key: bfloat16 [2048, 1024], P(None, 'tp'), may hold values from -0.125 to 0.125
- w_value: bfloat16 [2048, 1024], P(None, 'tp'), may hold values from -0.125 to 0.125
- w_output_gate: bfloat16 [2048, 1024], P(None, 'tp'), may hold values from -0.125 to 0.125
- w_decay: bfloat16 [2048, 16], replicated, may hold values from -0.125 to 0.125
- w_beta: bfloat16 [2048, 16], replicated, may hold values from -0.125 to 0.125
- decay_rate: float32 [16], P('tp'), may hold values from 0.1 to 2
- decay_shift: float32 [16], P('tp'), may hold values from -2 to 1
- head_gain: float32 [64], replicated, may hold values from 0.1 to 1.9
- w_mix_out: bfloat16 [1024, 2048], P(None, 'tp'), may hold values from -0.1875 to 0.1875
- expert_ids: int32 [512, 2], P('ep'), may hold values from 0 to 7, all different within a row; in each aligned block of 64 rows (0 to 63, 64 to 127, ...) at most 32 rows name the same one
- expert_weights: float32 [512, 2], P('ep'), may hold values from 0.2 to 1
- w_gate: bfloat16 [8, 2048, 4096], P('ep', None, 'tp'), may hold values from -0.125 to 0.125
- w_up: bfloat16 [8, 2048, 4096], P('ep', None, 'tp'), may hold values from -0.125 to 0.125
- w_down: bfloat16 [8, 4096, 2048], P('ep', 'tp'), may hold values from -0.09375 to 0.09375
Outputs:
- layer_out: bfloat16 [512, 2048], P('ep', 'tp')
- new_state: float32 [512, 16, 64, 64], P('ep', 'tp')
Inputs may be any that keep to these rules, and one draw needn't show every extreme that they name: `expert_ids`: each row names 2 different experts; within the rows of one index of ep (aligned blocks of 64 rows) no expert is named by more than 32 rows, and in some blocks one expert is named by exactly 32 rows.
All inputs are finite; a program needn't handle non-finite values.
Results may differ from a plain program's by a relative error of at most 0.013.
Values may be sent and summed in bfloat16 or wider, within the bound.
A program may use at most 64 MiB of HBM per device.

v0:
```python
import jax
import jax.numpy as jnp
from jax import lax
from jax.sharding import PartitionSpec as P

EPS = 1e-06


def unit_norm(values):
    return values * lax.rsqrt(jnp.sum(values * values, axis=-1, keepdims=True) + EPS)


def stored(values):
    return lax.optimization_barrier(values.astype(jnp.bfloat16)).astype(jnp.float32)


def shards(
    tokens,
    state,
    attn_gain,
    ffn_gain,
    w_query,
    w_key,
    w_value,
    w_output_gate,
    w_decay,
    w_beta,
    decay_rate,
    decay_shift,
    head_gain,
    w_mix_out,
    expert_ids,
    expert_weights,
    w_gate,
    w_up,
    w_down,
):
    groups = lax.axis_size("ep")
    seq_count = tokens.shape[0]
    own_width = tokens.shape[1]
    model_width = ffn_gain.shape[0]
    head_dim = head_gain.shape[0]
    heads_here = decay_rate.shape[0]
    top_count = expert_ids.shape[1]
    local_experts = w_gate.shape[0]
    expert_total = local_experts * groups
    capacity = max(2, 2 * seq_count * top_count // expert_total)
    whole_rows = lax.all_gather(tokens, "tp", axis=1, tiled=True)
    whole_f32 = whole_rows.astype(jnp.float32)
    normed = (
        whole_f32
        * lax.rsqrt(jnp.mean(whole_f32 * whole_f32, axis=1, keepdims=True) + EPS)
        * attn_gain
    ).astype(jnp.bfloat16)

    def project(weight):
        return jnp.dot(normed, weight, preferred_element_type=jnp.float32)

    def by_head(values):
        return values.reshape(seq_count, heads_here, head_dim)

    first_head = lax.axis_index("tp") * heads_here
    decay_cols = lax.dynamic_slice_in_dim(w_decay, first_head, heads_here, 1)
    beta_cols = lax.dynamic_slice_in_dim(w_beta, first_head, heads_here, 1)
    query_proj = stored(project(w_query))
    key_proj = stored(project(w_key))
    value_proj = stored(project(w_value))
    gate_proj = stored(project(w_output_gate))
    keep_rate = jnp.exp(-decay_rate * jax.nn.softplus(project(decay_cols) + decay_shift))
    beta_gate = jax.nn.sigmoid(project(beta_cols))
    query_head = unit_norm(jax.nn.silu(by_head(query_proj))) * head_dim ** (-0.5)
    key_head = unit_norm(jax.nn.silu(by_head(key_proj)))
    value_head = jax.nn.silu(by_head(value_proj))
    decayed = keep_rate[:, :, None, None] * state
    recalled = jnp.einsum("thd,thde->the", key_head, decayed, precision=lax.Precision.HIGHEST)
    correction = beta_gate[:, :, None] * (value_head - recalled)
    new_state = decayed + key_head[:, :, :, None] * correction[:, :, None, :]
    reading = jnp.einsum("thd,thde->the", query_head, new_state, precision=lax.Precision.HIGHEST)
    reading_scale = lax.rsqrt(jnp.mean(reading * reading, axis=-1, keepdims=True) + EPS)
    head_out = (reading * reading_scale * head_gain * jax.nn.silu(by_head(gate_proj))).astype(
        jnp.bfloat16
    )
    head_out = head_out.reshape(seq_count, heads_here * head_dim)
    mixed = jnp.dot(
        lax.all_gather(head_out, "tp", axis=1, tiled=True),
        w_mix_out,
        preferred_element_type=jnp.float32,
    )
    residual = (tokens.astype(jnp.float32) + mixed).astype(jnp.bfloat16)
    residual_f32 = residual.astype(jnp.float32)
    pair_count = seq_count * top_count
    flat_ids = expert_ids.reshape(pair_count)
    one_hot = (flat_ids[:, None] == jnp.arange(expert_total, dtype=jnp.int32)[None, :]).astype(
        jnp.int32
    )
    pair_index = jnp.arange(pair_count, dtype=jnp.int32)
    lower_mask = (pair_index[:, None] > pair_index[None, :]).astype(jnp.int32)
    earlier = jnp.dot(lower_mask, one_hot)
    slot_rank = jnp.sum(earlier * one_hot, axis=1)
    slot_of = flat_ids * capacity + slot_rank
    slot_count = expert_total * capacity
    slot_hit = jnp.arange(slot_count, dtype=jnp.int32)[:, None] == slot_of[None, :]
    dispatch = slot_hit.astype(jnp.bfloat16)
    dispatch_tokens = jnp.any(slot_hit.reshape(slot_count, seq_count, top_count), axis=2).astype(
        jnp.bfloat16
    )
    own_gain = lax.dynamic_slice_in_dim(ffn_gain, lax.axis_index("tp") * own_width, own_width, 0)
    square_total = lax.psum(jnp.sum(residual_f32 * residual_f32, axis=1), "tp")
    row_scale = lax.rsqrt(square_total / model_width + EPS)
    normed_ffn = (residual_f32 * row_scale[:, None] * own_gain).astype(jnp.bfloat16)
    outgoing = jnp.dot(dispatch_tokens, normed_ffn, preferred_element_type=jnp.float32).astype(
        jnp.bfloat16
    )
    arrived = lax.all_to_all(outgoing, "ep", split_axis=0, concat_axis=0, tiled=True)
    segment = lax.all_gather(arrived, "tp", axis=1, tiled=True)
    blocks = segment.reshape(groups, local_experts, capacity, segment.shape[1])
    gate_part = jnp.einsum("secd,edf->secf", blocks, w_gate, preferred_element_type=jnp.float32)
    up_part = jnp.einsum("secd,edf->secf", blocks, w_up, preferred_element_type=jnp.float32)
    expert_hidden = (jax.nn.silu(gate_part) * up_part).astype(jnp.bfloat16)
    partial_value = jnp.einsum(
        "secf,efd->secd", expert_hidden, w_down, preferred_element_type=jnp.float32
    )
    partial_value = partial_value.astype(jnp.bfloat16).reshape(
        groups * local_experts * capacity, model_width
    )
    summed = lax.psum_scatter(
        partial_value.astype(jnp.float32).astype(jnp.bfloat16),
        "tp",
        scatter_dimension=1,
        tiled=True,
    )
    returned = lax.all_to_all(summed, "ep", split_axis=0, concat_axis=0, tiled=True)
    pair_rows = jnp.einsum("sp,sd->pd", dispatch, returned, preferred_element_type=jnp.float32)
    weighted = jnp.sum(
        pair_rows.reshape(seq_count, top_count, own_width) * expert_weights[:, :, None], axis=1
    )
    layer_out = (residual_f32 + weighted).astype(jnp.bfloat16)
    return (layer_out, new_state)


def solution(mesh):
    in_specs = (
        P("ep", "tp"),
        P("ep", "tp", None, None),
        P(),
        P(),
        P(None, "tp"),
        P(None, "tp"),
        P(None, "tp"),
        P(None, "tp"),
        P(),
        P(),
        P("tp"),
        P("tp"),
        P(),
        P(None, "tp"),
        P("ep", None),
        P("ep", None),
        P("ep", None, "tp"),
        P("ep", None, "tp"),
        P("ep", "tp", None),
    )
    out_specs = (P("ep", "tp"), P("ep", "tp", None, None))
    return jax.shard_map(shards, mesh=mesh, in_specs=in_specs, out_specs=out_specs, check_vma=False)
```

profile of v0, /device:TPU:0, one launch (start us, length us, event | category | flops | bytes accessed | tf_op | source)
XLA Modules:
  0.0 171.2 jit_solution(3074201662367445162)
XLA Ops:
  7.2 10.9 %all_gather.9 = bf16[64,2048]{1,0:T(8,128)(2,1)S(1)} all-gather(bf16[64,512]{1,0:T(8,128)(2,1)} %param.19), channel_id=1, replica_groups=mesh['ep'=8,'tp'=4] {'tp'}, dimensions={1}, use_global_device_ids=true | all-gather | bytes 327680 | tf_op jit(solution)/shard_map/all_gather | solution.py:48
  18.1 0.2 fusion.36
  18.3 1.6 convolution_convert_fusion.3
  19.9 0.1 reshape.179
  20.0 0.2 multiply_reduce_fusion.2
  20.2 0.1 broadcast_multiply_fusion
  20.3 0.7 neg.32
  21.0 1.0 fusion.51
  22.0 0.1 copy.39
  22.1 1.0 fusion.33
  23.2 0.1 copy.40
  23.3 1.6 convolution_convert_fusion.2
  24.9 0.1 reshape.181
  25.0 10.1 %fusion = f32[64,4,1,64]{3,2,1,0:T(1,128)S(1)} fusion(f32[64,4,64,1]{2,3,1,0:T(1,128)S(1)} %bitcast.87, f32[64,4,64,64]{3,2,1,0:T(8,128)} %param.20, f32[64,4]{1,0:T(8,128)S(1)} %copy.39), kind=kOutput, calls=%fused_computation.1 | convolution fusion | flops 13631488 | bytes 4326400 | tf_op jit(solution)/shard_map/thd,thde->the/dot_general | solution.py:75
  35.1 0.1 fusion.42
  35.3 5.2 %multiply_add_fusion = f32[64,4,64,64]{3,2,1,0:T(8,128)} fusion(f32[64,4,64,64]{3,2,1,0:T(8,128)S(1)} %copy-done.1, f32[64,4,64]{2,1,0:T(4,128)S(1)} %fusion.42, f32[64,4,64]{2,1,0:T(4,128)S(1)} %broadcast_multiply_fusion, f32[64,4]{1,0:T(8,128)S(1)} %copy.39), kind=kLoop, calls=%fused_computation | loop fusion | flops 3145728 | bytes 8520704 | tf_op jit(solution)/shard_map/add | solution.py:77
  40.6 0.3 convolution_convert_fusion.4
  40.9 0.1 reshape.177
  41.0 0.2 multiply_reduce_fusion.3
  41.2 0.1 multiply_multiply_fusion
  41.4 9.5 %fusion.64 = f32[64,4,1,64]{3,2,1,0:T(1,128)S(1)} fusion(f32[64,4,64,1]{2,3,1,0:T(1,128)S(1)} %bitcast.95, f32[64,4,64,64]{3,2,1,0:T(8,128)} %multiply_add_fusion), kind=kOutput, calls=%fused_computation.79 | convolution fusion | flops 12582912 | bytes 4325376 | tf_op jit(solution)/shard_map/thd,thde->the/dot_general | solution.py:78
  50.9 0.1 multiply_reduce_fusion.1
  51.0 0.3 convolution_convert_fusion.1
  51.4 0.1 reshape.183
  51.5 0.1 fusion.44
  51.7 0.1 reshape.168
  51.8 8.7 %all_gather.10 = bf16[64,1024]{1,0:T(8,128)(2,1)S(1)} all-gather(bf16[64,256]{1,0:T(8,128)(2,1)S(1)} %reshape.168), channel_id=1, replica_groups=mesh['ep'=8,'tp'=4] {'tp'}, dimensions={1}, use_global_device_ids=true | all-gather | bytes 163840 | tf_op jit(solution)/shard_map/all_gather | solution.py:85
  60.5 0.4 multiply_reduce_fusion
  60.9 8.9 %psum.7 = f32[64]{0:T(128)S(1)} all-reduce(f32[64]{0:T(128)S(1)} %get-tuple-element.2), channel_id=1, replica_groups=mesh['ep'=8,'tp'=4] {'tp'}, use_global_device_ids=true, to_apply=%region_7.8 | all-reduce | flops 64 | bytes 512 | tf_op jit(solution)/shard_map/psum | solution.py:108
  69.8 0.1 copy.41
  69.9 0.1 reshape.169
  70.0 0.1 fusion.30
  70.2 0.2 reduce_sum.70
  70.4 0.1 copy.42
  70.4 0.1 fusion.43
  70.6 0.8 dynamic_slice.11
  71.3 0.3 convolution_convert_fusion
  71.6 14.5 %all_to_all.24 = bf16[8,32,512]{2,1,0:T(8,128)(2,1)} all-to-all(bf16[8,32,512]{2,1,0:T(8,128)(2,1)S(1)} %bitcast.90), channel_id=1, replica_groups=mesh['ep'=8,'tp'=4] {'ep'}, dimensions={0} | all-to-all | bytes 524288 | tf_op jit(solution)/shard_map/all_to_all | solution.py:114
  86.1 0.0 reduce-scatter.2.cloned.1.call-start
  86.2 23.8 %all-gather.2.cloned.1.call-done = bf16[256,2048]{1,0:T(8,128)(2,1)} async-done(((bf16[256,512]{1,0:T(8,128)(2,1)}), bf16[256,2048]{1,0:T(8,128)(2,1)}) %all-gather.2.cloned.1.call-update) | async-done | bytes 1048592 | tf_op jit(solution)/shard_map/all_gather | solution.py:115
  110.0 3.8 %fusion.12 = f32[8,1,32,1024]{3,2,0,1:T(8,128)S(1)} fusion(bf16[8,32,2048]{2,1,0:T(8,128)(2,1)} %bitcast.97, bf16[1,2048,1024]{2,1,0:T(8,128)(2,1)} %param.35), kind=kOutput, calls=%fused_computation.11 | convolution fusion | flops 1073741824 | bytes 6291456 | tf_op jit(solution)/shard_map/secd,edf->secf/dot_general | solution.py:117
  113.7 7.4 %fusion.9 = bf16[8,32,2048]{2,1,0:T(8,128)(2,1)} fusion(bf16[1,1024,2048]{2,1,0:T(8,128)(2,1)} %param.37, bf16[8,32,2048]{2,1,0:T(8,128)(2,1)} %bitcast.98, bf16[1,2048,1024]{2,1,0:T(8,128)(2,1)} %param.36, f32[8,1,32,1024]{3,2,0,1:T(8,128)S(1)} %fusion.12), kind=kOutput, calls=%fused_computation.10 | convolution fusion | flops 2149580800 | bytes 11534336 | tf_op jit(solution)/shard_map/secf,efd->secd/dot_general | solution.py:120
  121.1 28.1 %reduce-scatter.2.cloned.1.call-done = bf16[256,512]{1,0:T(8,128)(2,1)} async-done(((bf16[256,2048]{1,0:T(8,128)(2,1)}), bf16[256,512]{1,0:T(8,128)(2,1)}) %reduce-scatter.2.cloned.1.call-update) | async-done | bytes 262160 | tf_op jit(solution)/shard_map/reduce_scatter | solution.py:126
  149.2 4.6 %all-to-all-start.1 = ((bf16[8,32,512]{2,1,0:T(8,128)(2,1)}), bf16[8,32,512]{2,1,0:T(8,128)(2,1)S(1)}, u32[]{:S(2)}, u32[]{:S(2)}) async-start(bf16[8,32,512]{2,1,0:T(8,128)(2,1)} %bitcast.96), calls=%async_computation.2 | async-start | bytes 524288 | tf_op jit(solution)/shard_map/all_to_all | solution.py:132
  153.8 0.1 iota_compare_fusion.1
  154.0 9.6 %all-to-all-done.1 = bf16[8,32,512]{2,1,0:T(8,128)(2,1)S(1)} async-done(((bf16[8,32,512]{2,1,0:T(8,128)(2,1)}), bf16[8,32,512]{2,1,0:T(8,128)(2,1)S(1)}, u32[]{:S(2)}, u32[]{:S(2)}) %all-to-all-start.1) | async-done | bytes 262176 | tf_op jit(solution)/shard_map/all_to_all | solution.py:132
  163.5 0.2 fusion.27
  163.7 0.7 add_convert_fusion
  (29 shorter events, 0.2 us)
Async XLA Ops:
  7.2 53.3 %copy-start = (bf16[1024,512]{1,0:T(8,128)(2,1)S(1)}, bf16[1024,512]{1,0:T(8,128)(2,1)}, u32[]{:S(2)}) copy-start(bf16[1024,512]{1,0:T(8,128)(2,1)} %param.32) | copy-start | bytes 3145732
  7.2 102.8 %all-gather.2.cloned.1.call-start = ((), (), s32[]{:S(2)}) async-start(), calls=%async_computation.3 | async-start | bytes 1310720 | tf_op jit(solution)/shard_map/all_gather | solution.py:115
  25.0 10.3 %copy-start.1 = (f32[64,4,64,64]{3,2,1,0:T(8,128)S(1)}, f32[64,4,64,64]{3,2,1,0:T(8,128)}, u32[]{:S(2)}) copy-start(f32[64,4,64,64]{3,2,1,0:T(8,128)} %param.20) | copy-start | bytes 12582916
  35.3 5.2 %copy-start.2 = (bf16[2048,256]{1,0:T(8,128)(2,1)S(1)}, bf16[2048,256]{1,0:T(8,128)(2,1)}, u32[]{:S(2)}) copy-start(bf16[2048,256]{1,0:T(8,128)(2,1)} %param.23) | copy-start | bytes 3145732
  35.3 5.2 %copy-start.5 = (f32[2048]{0:T(1024)S(1)}, f32[2048]{0:T(1024)}, u32[]{:S(2)}) copy-start(f32[2048]{0:T(1024)} %param.21) | copy-start | bytes 24580
  40.5 10.5 %copy-start.3 = (bf16[2048,256]{1,0:T(8,128)(2,1)S(1)}, bf16[2048,256]{1,0:T(8,128)(2,1)}, u32[]{:S(2)}) copy-start(bf16[2048,256]{1,0:T(8,128)(2,1)} %param.26) | copy-start | bytes 3145732
  40.5 11.0 %copy-start.8 = (f32[64]{0:T(128)S(1)}, f32[64]{0:T(128)}, u32[]{:S(2)}) copy-start(f32[64]{0:T(128)} %param.31) | copy-start | bytes 772
  40.5 19.9 %copy-start.4 = (bf16[64,512]{1,0:T(8,128)(2,1)S(1)}, bf16[64,512]{1,0:T(8,128)(2,1)}, u32[]{:S(2)}) copy-start(bf16[64,512]{1,0:T(8,128)(2,1)} %param.19) | copy-start | bytes 196612
  40.5 29.3 %copy-start.6 = (s32[64,2]{0,1:T(2,128)S(1)}, s32[64,2]{0,1:T(2,128)}, u32[]{:S(2)}) copy-start(s32[64,2]{0,1:T(2,128)} %param.33) | copy-start | bytes 1540
  86.1 63.1 %reduce-scatter.2.cloned.1.call-start = ((), (), s32[]{:S(2)}) async-start(), calls=%async_computation.4 | async-start | bytes 1310720 | tf_op jit(solution)/shard_map/reduce_scatter | solution.py:126
  113.7 49.8 %copy-start.7 = (f32[64,2]{0,1:T(2,128)S(1)}, f32[64,2]{0,1:T(2,128)}, u32[]{:S(2)}) copy-start(f32[64,2]{0,1:T(2,128)} %param.34) | copy-start | bytes 1540
  149.2 14.3 %all-to-all-start.1 = ((bf16[8,32,512]{2,1,0:T(8,128)(2,1)}), bf16[8,32,512]{2,1,0:T(8,128)(2,1)S(1)}, u32[]{:S(2)}, u32[]{:S(2)}) async-start(bf16[8,32,512]{2,1,0:T(8,128)(2,1)} %bitcast.96), calls=%async_computation.2 | async-start | bytes 524288 | tf_op jit(solution)/shard_map/all_to_all | solution.py:132
Sparse Core Ops, SparseCore 0:
  86.2 23.6 all-gather.1
  121.2 27.9 reduce-scatter.1
where the time goes:
time: 172 us; the launch traced here: 171 us
  waiting for transfers between devices  61.5 us (36%)
  blocking collectives  43 us (25%)
  matrix products  37.7 us (22%)
  between operations  14.3 us (8%)
  other arithmetic  7.97 us (5%)
  starting transfers between devices  4.68 us (3%)
  local copies, waits for them, and re-layouts  2.11 us (1%)
    reduce_scatter x1, waiting for transfers between devices, shards(): lax.psum_scatter(partial_value.astype(jnp.float32).astype(jnp.bfloat16),...  28.1 us
    all_gather x1, waiting for transfers between devices, shards(): segment = lax.all_gather(arrived, 'tp', axis=1, tiled=True)  23.8 us
    all_to_all x1, blocking collectives, shards(): lax.all_to_all(outgoing, 'ep', split_axis=0, concat_axis=0, tiled=True)  14.5 us
    all_gather x1, blocking collectives, shards(): whole_rows = lax.all_gather(tokens, 'tp', axis=1, tiled=True)  10.9 us
    dot_general x1, matrix products, shards(): jnp.einsum('thd,thde->the', key_head, decayed, precision=lax.Precision.HI...  10.1 us
    all_to_all x1, waiting for transfers between devices, shards(): lax.all_to_all(summed, 'ep', split_axis=0, concat_axis=0, tiled=True)  9.56 us
    dot_general x1, matrix products, shards(): jnp.einsum('thd,thde->the', query_head, new_state, precision=lax.Precisio...  9.48 us
    psum x1, blocking collectives, shards(): square_total = lax.psum(jnp.sum(residual_f32 * residual_f32, axis=1), 'tp')  8.93 us
  transfers between devices with their start and end apart: 3, of which 3 were waited for; matrix products, arithmetic and copies ran while one was open for 0% of the time, Pallas kernels for 0%

commit v1 on v0

--- a/solution.py
+++ b/solution.py
@@ -4,6 +4,11 @@
 from jax.sharding import PartitionSpec as P
 
 EPS = 1e-06
+
+
+def gather_and_add(shard, name):
+    terms = lax.all_gather(shard, name)
+    return jnp.sum(terms, axis=0)
 
 
 def unit_norm(values):
@@ -105,7 +110,7 @@
         jnp.bfloat16
     )
     own_gain = lax.dynamic_slice_in_dim(ffn_gain, lax.axis_index("tp") * own_width, own_width, 0)
-    square_total = lax.psum(jnp.sum(residual_f32 * residual_f32, axis=1), "tp")
+    square_total = gather_and_add(jnp.sum(residual_f32 * residual_f32, axis=1), "tp")
     row_scale = lax.rsqrt(square_total / model_width + EPS)
     normed_ffn = (residual_f32 * row_scale[:, None] * own_gain).astype(jnp.bfloat16)
     outgoing = jnp.dot(dispatch_tokens, normed_ffn, preferred_element_type=jnp.float32).astype(

time: 172 us -> 174 us (1.012)
    unnamed x0 -> x1, blocking collectives: none -> 9.07 us
    psum x1 -> x0, blocking collectives: 8.93 us -> none  [shards(): square_total = lax.psum(jnp.sum(residual_f32 * residual_f32, axis=1), 'tp')]
where the time goes in v1:
time: 174 us; the launch traced here: 173 us
  waiting for transfers between devices  61.5 us (35%)
  blocking collectives  43.1 us (25%)
  matrix products  37.6 us (22%)
  between operations  15 us (9%)
  other arithmetic  8.03 us (5%)
  starting transfers between devices  4.68 us (3%)
  local copies, waits for them, and re-layouts  3.03 us (2%)
    reduce_scatter x1, waiting for transfers between devices, shards(): lax.psum_scatter(partial_value.astype(jnp.float32).astype(jnp.bfloat16),...  28.1 us
    all_gather x1, waiting for transfers between devices, shards(): segment = lax.all_gather(arrived, 'tp', axis=1, tiled=True)  23.8 us
    all_to_all x1, blocking collectives, shards(): lax.all_to_all(outgoing, 'ep', split_axis=0, concat_axis=0, tiled=True)  14.5 us
    all_gather x1, blocking collectives, shards(): whole_rows = lax.all_gather(tokens, 'tp', axis=1, tiled=True)  10.9 us
    dot_general x1, matrix products, shards(): jnp.einsum('thd,thde->the', key_head, decayed, precision=lax.Precision.HI...  10.1 us
    all_to_all x1, waiting for transfers between devices, shards(): lax.all_to_all(summed, 'ep', split_axis=0, concat_axis=0, tiled=True)  9.56 us
    dot_general x1, matrix products, shards(): jnp.einsum('thd,thde->the', query_head, new_state, precision=lax.Precisio...  9.48 us
    unnamed x1, blocking collectives  9.07 us
  transfers between devices with their start and end apart: 3, of which 3 were waited for; matrix products, arithmetic and copies ran while one was open for 0% of the time, Pallas kernels for 0%

profile of v1, /device:TPU:0, one launch (start us, length us, event | category | flops | bytes accessed | tf_op | source)
XLA Modules:
  0.0 173.0 jit_solution(3734806167504415430)
XLA Ops:
  7.2 10.9 %all_gather.15 = bf16[64,2048]{1,0:T(8,128)(2,1)S(1)} all-gather(bf16[64,512]{1,0:T(8,128)(2,1)} %param.19), channel_id=1, replica_groups=mesh['ep'=8,'tp'=4] {'tp'}, dimensions={1}, use_global_device_ids=true | all-gather | bytes 327680 | tf_op jit(solution)/shard_map/all_gather | solution.py:53
  18.1 0.2 fusion.36
  18.3 1.6 convolution_convert_fusion.3
  19.9 0.1 reshape.183
  20.0 0.2 multiply_reduce_fusion.2
  20.2 0.1 broadcast_multiply_fusion
  20.3 0.7 neg.32
  21.0 1.0 fusion.51
  22.0 0.1 copy.39
  22.1 1.0 fusion.33
  23.2 0.1 copy.40
  23.3 1.6 convolution_convert_fusion.2
  24.9 0.1 reshape.185
  25.0 10.1 %fusion = f32[64,4,1,64]{3,2,1,0:T(1,128)S(1)} fusion(f32[64,4,64,1]{2,3,1,0:T(1,128)S(1)} %bitcast.88, f32[64,4,64,64]{3,2,1,0:T(8,128)} %param.20, f32[64,4]{1,0:T(8,128)S(1)} %copy.39), kind=kOutput, calls=%fused_computation.1 | convolution fusion | flops 13631488 | bytes 4326400 | tf_op jit(solution)/shard_map/thd,thde->the/dot_general | solution.py:80
  35.1 0.1 fusion.42
  35.3 5.2 %multiply_add_fusion = f32[64,4,64,64]{3,2,1,0:T(8,128)} fusion(f32[64,4,64,64]{3,2,1,0:T(8,128)S(1)} %copy-done.1, f32[64,4,64]{2,1,0:T(4,128)S(1)} %fusion.42, f32[64,4,64]{2,1,0:T(4,128)S(1)} %broadcast_multiply_fusion, f32[64,4]{1,0:T(8,128)S(1)} %copy.39), kind=kLoop, calls=%fused_computation | loop fusion | flops 3145728 | bytes 8520704 | tf_op jit(solution)/shard_map/add | solution.py:82
  40.6 0.3 convolution_convert_fusion.4
  41.0 0.1 reshape.181
  41.1 0.2 multiply_reduce_fusion.3
  41.3 0.1 multiply_multiply_fusion
  41.4 9.5 %fusion.64 = f32[64,4,1,64]{3,2,1,0:T(1,128)S(1)} fusion(f32[64,4,64,1]{2,3,1,0:T(1,128)S(1)} %bitcast.96, f32[64,4,64,64]{3,2,1,0:T(8,128)} %multiply_add_fusion), kind=kOutput, calls=%fused_computation.79 | convolution fusion | flops 12582912 | bytes 4325376 | tf_op jit(solution)/shard_map/thd,thde->the/dot_general | solution.py:83
  50.9 0.1 multiply_reduce_fusion.1
  51.1 0.3 convolution_convert_fusion.1
  51.4 0.1 reshape.187
  51.6 0.1 fusion.44
  51.7 0.1 reshape.172
  51.8 8.7 %all_gather.16 = bf16[64,1024]{1,0:T(8,128)(2,1)S(1)} all-gather(bf16[64,256]{1,0:T(8,128)(2,1)S(1)} %reshape.172), channel_id=1, replica_groups=mesh['ep'=8,'tp'=4] {'tp'}, dimensions={1}, use_global_device_ids=true | all-gather | bytes 163840 | tf_op jit(solution)/shard_map/all_gather | solution.py:90
  60.5 0.4 multiply_reduce_fusion
  60.9 0.6 dynamic-slice
  62.2 0.2 dynamic-update-slice
  62.4 9.1 %all-reduce = f32[256]{0:T(256)S(1)} all-reduce(f32[256]{0:T(256)S(1)} %dynamic-update-slice), channel_id=2, replica_groups=mesh['ep'=8,'tp'=4] {'tp'}, use_global_device_ids=true, to_apply=%add | all-reduce | flops 256 | bytes 2048
  71.6 0.1 copy.41
  71.7 0.1 reshape.173
  71.8 0.1 fusion.30
  72.0 0.2 reduce_sum.79
  72.2 0.1 fusion.43
  72.3 0.8 dynamic_slice.11
  73.1 0.3 convolution_convert_fusion
  73.4 14.5 %all_to_all.24 = bf16[8,32,512]{2,1,0:T(8,128)(2,1)} all-to-all(bf16[8,32,512]{2,1,0:T(8,128)(2,1)S(1)} %bitcast.91), channel_id=1, replica_groups=mesh['ep'=8,'tp'=4] {'ep'}, dimensions={0} | all-to-all | bytes 524288 | tf_op jit(solution)/shard_map/all_to_all | solution.py:119
  88.0 23.8 %all-gather.3.cloned.1.call-done = bf16[256,2048]{1,0:T(8,128)(2,1)} async-done(((bf16[256,512]{1,0:T(8,128)(2,1)}), bf16[256,2048]{1,0:T(8,128)(2,1)}) %all-gather.3.cloned.1.call-update) | async-done | bytes 1048592 | tf_op jit(solution)/shard_map/all_gather | solution.py:120
  111.8 3.8 %fusion.12 = f32[8,1,32,1024]{3,2,0,1:T(8,128)S(1)} fusion(bf16[8,32,2048]{2,1,0:T(8,128)(2,1)} %bitcast.98, bf16[1,2048,1024]{2,1,0:T(8,128)(2,1)} %param.35), kind=kOutput, calls=%fused_computation.11 | convolution fusion | flops 1073741824 | bytes 6291456 | tf_op jit(solution)/shard_map/secd,edf->secf/dot_general | solution.py:122
  115.5 7.4 %fusion.9 = bf16[8,32,2048]{2,1,0:T(8,128)(2,1)} fusion(bf16[1,1024,2048]{2,1,0:T(8,128)(2,1)} %param.37, bf16[8,32,2048]{2,1,0:T(8,128)(2,1)} %bitcast.99, bf16[1,2048,1024]{2,1,0:T(8,128)(2,1)} %param.36, f32[8,1,32,1024]{3,2,0,1:T(8,128)S(1)} %fusion.12), kind=kOutput, calls=%fused_computation.10 | convolution fusion | flops 2149580800 | bytes 11534336 | tf_op jit(solution)/shard_map/secf,efd->secd/dot_general | solution.py:125
  122.9 28.1 %reduce-scatter.2.cloned.1.call-done = bf16[256,512]{1,0:T(8,128)(2,1)} async-done(((bf16[256,2048]{1,0:T(8,128)(2,1)}), bf16[256,512]{1,0:T(8,128)(2,1)}) %reduce-scatter.2.cloned.1.call-update) | async-done | bytes 262160 | tf_op jit(solution)/shard_map/reduce_scatter | solution.py:131
  151.0 4.6 %all-to-all-start.1 = ((bf16[8,32,512]{2,1,0:T(8,128)(2,1)}), bf16[8,32,512]{2,1,0:T(8,128)(2,1)S(1)}, u32[]{:S(2)}, u32[]{:S(2)}) async-start(bf16[8,32,512]{2,1,0:T(8,128)(2,1)} %bitcast.97), calls=%async_computation.2 | async-start | bytes 524288 | tf_op jit(solution)/shard_map/all_to_all | solution.py:137
  155.6 0.1 iota_compare_fusion.1
  155.8 9.6 %all-to-all-done.1 = bf16[8,32,512]{2,1,0:T(8,128)(2,1)S(1)} async-done(((bf16[8,32,512]{2,1,0:T(8,128)(2,1)}), bf16[8,32,512]{2,1,0:T(8,128)(2,1)S(1)}, u32[]{:S(2)}, u32[]{:S(2)}) %all-to-all-start.1) | async-done | bytes 262176 | tf_op jit(solution)/shard_map/all_to_all | solution.py:137
  165.3 0.2 fusion.27
  165.5 0.7 add_convert_fusion
  (36 shorter events, 0.5 us)
Async XLA Ops:
  7.2 53.4 %copy-start = (bf16[1024,512]{1,0:T(8,128)(2,1)S(1)}, bf16[1024,512]{1,0:T(8,128)(2,1)}, u32[]{:S(2)}) copy-start(bf16[1024,512]{1,0:T(8,128)(2,1)} %param.32) | copy-start | bytes 3145732
  7.2 104.6 %all-gather.3.cloned.1.call-start = ((), (), s32[]{:S(2)}) async-start(), calls=%async_computation.3 | async-start | bytes 1310720 | tf_op jit(solution)/shard_map/all_gather | solution.py:120
  25.0 10.3 %copy-start.1 = (f32[64,4,64,64]{3,2,1,0:T(8,128)S(1)}, f32[64,4,64,64]{3,2,1,0:T(8,128)}, u32[]{:S(2)}) copy-start(f32[64,4,64,64]{3,2,1,0:T(8,128)} %param.20) | copy-start | bytes 12582916
  35.3 5.3 %copy-start.2 = (bf16[2048,256]{1,0:T(8,128)(2,1)S(1)}, bf16[2048,256]{1,0:T(8,128)(2,1)}, u32[]{:S(2)}) copy-start(bf16[2048,256]{1,0:T(8,128)(2,1)} %param.23) | copy-start | bytes 3145732
  35.3 5.3 %copy-start.5 = (f32[2048]{0:T(1024)S(1)}, f32[2048]{0:T(1024)}, u32[]{:S(2)}) copy-start(f32[2048]{0:T(1024)} %param.21) | copy-start | bytes 24580
  40.6 10.5 %copy-start.3 = (bf16[2048,256]{1,0:T(8,128)(2,1)S(1)}, bf16[2048,256]{1,0:T(8,128)(2,1)}, u32[]{:S(2)}) copy-start(bf16[2048,256]{1,0:T(8,128)(2,1)} %param.26) | copy-start | bytes 3145732
  40.6 11.0 %copy-start.8 = (f32[64]{0:T(128)S(1)}, f32[64]{0:T(128)}, u32[]{:S(2)}) copy-start(f32[64]{0:T(128)} %param.31) | copy-start | bytes 772
  40.6 19.9 %copy-start.4 = (bf16[64,512]{1,0:T(8,128)(2,1)S(1)}, bf16[64,512]{1,0:T(8,128)(2,1)}, u32[]{:S(2)}) copy-start(bf16[64,512]{1,0:T(8,128)(2,1)} %param.19) | copy-start | bytes 196612
  40.6 20.3 %copy-start.9 = (u32[32]{0:T(128)S(1)}, u32[32]{0:T(128)}, u32[]{:S(2)}) copy-start(u32[32]{0:T(128)} %constant.51) | copy-start | bytes 388
  40.6 31.0 %copy-start.6 = (s32[64,2]{0,1:T(2,128)S(1)}, s32[64,2]{0,1:T(2,128)}, u32[]{:S(2)}) copy-start(s32[64,2]{0,1:T(2,128)} %param.33) | copy-start | bytes 1540
  87.9 63.1 %reduce-scatter.2.cloned.1.call-start = ((), (), s32[]{:S(2)}) async-start(), calls=%async_computation.4 | async-start | bytes 1310720 | tf_op jit(solution)/shard_map/reduce_scatter | solution.py:131
  115.5 49.8 %copy-start.7 = (f32[64,2]{0,1:T(2,128)S(1)}, f32[64,2]{0,1:T(2,128)}, u32[]{:S(2)}) copy-start(f32[64,2]{0,1:T(2,128)} %param.34) | copy-start | bytes 1540
  151.0 14.3 %all-to-all-start.1 = ((bf16[8,32,512]{2,1,0:T(8,128)(2,1)}), bf16[8,32,512]{2,1,0:T(8,128)(2,1)S(1)}, u32[]{:S(2)}, u32[]{:S(2)}) async-start(bf16[8,32,512]{2,1,0:T(8,128)(2,1)} %bitcast.97), calls=%async_computation.2 | async-start | bytes 524288 | tf_op jit(solution)/shard_map/all_to_all | solution.py:137
Sparse Core Ops, SparseCore 0:
  88.0 23.6 all-gather.2
  123.0 27.9 reduce-scatter.1
